TPU v7x, 32 devices: a whole 2x2x4 slice. The times are simulated.
32 devices in a mesh: fs: 16 (over z, y, x), tp: 2 (over core).
Axes of the slice: x: 2, y: 2, z: 4, core: 2. Of those that a mesh axis runs over, the one named last changes fastest.
Arguments:
- tokens: bfloat16 [5120, 2048], P('fs'), may hold values from -6 to 6
- w_gate: bfloat16 [2048, 5632], P('fs', 'tp'), may hold values from -0.125 to 0.125
- w_up: bfloat16 [2048, 5632], P('fs', 'tp'), may hold values from -0.125 to 0.125
- w_down: bfloat16 [5632, 2048], P('tp', 'fs'), may hold values from -0.078125 to 0.078125
- w_mix_in: bfloat16 [2048, 1024], P('fs', 'tp'), may hold values from -0.125 to 0.125
- w_mix_out: bfloat16 [1024, 2048], P('tp', 'fs'), may hold values from -0.1875 to 0.1875
- pool_w: bfloat16 [8, 128, 128], P('tp'), may hold values from -0.5 to 0.5
- pool_scale: bfloat16 [1024], P('tp'), may hold values from 0.099609375 to 1.8984375
- norm_gains: float32 [6, 2048], replicated, may hold values from 0.1 to 1.9
Outputs:
- layer_out: bfloat16 [5120, 2048], P(('fs', 'tp'))
All inputs are finite; a program needn't handle non-finite values.
Results may differ from a plain program's by a relative error of at most 0.018.
Values may be sent and summed in bfloat16 or wider, within the bound.
A program may use at most 128 MiB of HBM per device.

v0:
```python
import functools
import itertools

import jax
import jax.numpy as jnp
from jax import lax
from jax.experimental import pallas as pl
from jax.experimental.pallas import tpu as pltpu
from jax.sharding import PartitionSpec as P

LEN = 64
MESH = pl.DeviceIdType.MESH


def line_dims(mesh):
    devices = mesh.devices.reshape(mesh.shape["fs"], -1)[:, 0]
    count = len(devices)
    coords = [tuple(getattr(d, "coords", ())) for d in devices]
    dims = []
    for axis in range(len(coords[0])):
        values = sorted({c[axis] for c in coords})
        if len(values) > 1:
            stride = next(i for i in range(count) if coords[i][axis] != coords[0][axis])
            dims.append((len(values), stride, axis, values))
    dims.sort(key=lambda d: -d[1])
    good = len(dims) > 0 and all(
        sum(vals.index(c[axis]) * stride for _, stride, axis, vals in dims) == i
        for i, c in enumerate(coords)
    )
    if not good:
        return ((count, 1),)
    return tuple((d[0], d[1]) for d in dims)


def near(position, size, rank):
    inner = jnp.minimum(position, size - 1 - position)
    alternating = rank <= 2 * inner
    distance = jnp.where(alternating, (rank + 1) // 2, rank - inner)
    toward_high = jnp.where(alternating, rank % 2 == 1, 2 * position < size - 1)
    step = jnp.where(toward_high, 1, -1)
    return position + step * distance, -step


def piece_plan(dims, order):
    sizes = [dims[d][0] for d in order]
    slots = []
    for ranks in itertools.product(*[range(n) for n in sizes]):
        slots.append(ranks)
    slots.sort(key=lambda r: (sum(r), r))
    return slots


class Piece:
    def __init__(self, index, dims, order, src_of, dst_of):
        self.index, self.dims, self.order = index, dims, order
        self.src_of, self.dst_of = src_of, dst_of
        self.slots = piece_plan(dims, order)

    def locate(self, me, ranks):
        source, last, away = me, -1, None
        for place, (d, rank) in enumerate(zip(self.order, ranks)):
            if rank > 0:
                size, stride = self.dims[d]
                position = (me // stride) % size
                found, step = near(position, size, rank)
                source = source + (found - position) * stride
                last, away = place, step
        return source, last, away

    def sends(self, me, ranks):
        _, last, away = self.locate(me, ranks)
        out = []
        for place, d in enumerate(self.order):
            size, stride = self.dims[d]
            position = (me // stride) % size
            if place == last:
                if size > 2:
                    ok = jnp.logical_and(position + away >= 0, position + away < size)
                    out.append((ok, me + away * stride))
            elif place > last:
                if size == 2:
                    out.append((None, me + (1 - 2 * position) * stride))
                else:
                    out.append((position + 1 < size, me + stride))
                    out.append((position > 0, me - stride))
        return out


def when(condition, act):
    if condition is None:
        act()
    else:
        pl.when(condition)(act)


def spread(pieces, me, chunk, send_sem, recv_sem, low, high, mode):
    todo = []
    for piece in pieces:
        for ranks in piece.slots:
            todo.append((sum(ranks), piece, ranks))
    todo.sort(key=lambda t: t[0])
    for depth, piece, ranks in todo:
        if not low <= depth < high:
            continue
        source, last, _ = piece.locate(me, ranks)
        landed = piece.dst_of(chunk, source)
        origin = piece.src_of(chunk) if depth == 0 else landed
        recv = recv_sem.at[chunk, piece.index, source]
        if depth > 0 and mode == "start":
            pltpu.make_async_copy(landed, landed, recv).wait()
        base = piece.first_send[ranks]
        for offset, (ok, target) in enumerate(piece.sends(me, ranks)):
            copy = pltpu.make_async_remote_copy(
                src_ref=origin,
                dst_ref=landed,
                send_sem=send_sem.at[chunk, base + offset],
                recv_sem=recv,
                device_id={"fs": target},
                device_id_type=MESH,
            )
            when(ok, copy.start if mode == "start" else copy.wait_send)


def number_sends(pieces):
    total = 0
    for piece in pieces:
        piece.first_send = {}
        for ranks in piece.slots:
            piece.first_send[ranks] = total
            last = max([i for i, r in enumerate(ranks) if r > 0], default=-1)
            for place, d in enumerate(piece.order):
                size = piece.dims[d][0]
                if place == last:
                    total += 1 if size > 2 else 0
                elif place > last:
                    total += 1 if size == 2 else 2
    return total


def cut(extent, unit, share):
    return max(unit, min(extent - unit, round(extent * share / unit) * unit))


def gather_plan(dims, refs, outs, blocks):
    gate, up, down, mix_in, mix_out = refs
    gate_o, up_o, down_o, mix_in_o, mix_out_o = outs
    n = len(dims)
    first = tuple(range(n))
    second = first[1:] + first[:1]
    third = first[-1:] + first[:-1]
    pooled = mix_out.shape[0]

    def rows(ref, out, start_of, size):
        return (
            lambda c: ref.at[pl.ds(start_of(c), size), :],
            lambda c, s: out.at[s, pl.ds(start_of(c), size), :],
        )

    def at(block, offset):
        return lambda c: pl.multiple_of(c * block + offset, 16)

    block, tall = gate.shape[0] // blocks, down.shape[0] // blocks
    down_cut = cut(tall, 16, 2 / 3)
    main = [
        Piece(0, dims, first, *rows(gate, gate_o, at(block, 0), block)),
        Piece(1, dims, third, *rows(up, up_o, at(block, 0), block)),
        Piece(2, dims, first, *rows(down, down_o, at(tall, 0), down_cut)),
        Piece(3, dims, second, *rows(down, down_o, at(tall, down_cut), tall - down_cut)),
    ]
    mix_cut = cut(pooled, 16, 2 / 3)

    def fixed(offset):
        return lambda c: offset

    mix = [
        Piece(0, dims, first, *rows(mix_in, mix_in_o, fixed(0), mix_in.shape[0])),
        Piece(1, dims, third, *rows(mix_out, mix_out_o, fixed(0), mix_cut)),
        Piece(2, dims, second, *rows(mix_out, mix_out_o, fixed(mix_cut), pooled - mix_cut)),
    ]
    return main, mix


def gather_kernel(dims, blocks, *args):
    refs, outs = args[:5], args[5:10]
    beside = None
    if len(args) > 13:
        beside = args[10:12]
        args = args[:10] + args[12:]
    send_sem, recv_sem, local_sem = args[10:13]
    me = lax.axis_index("fs")
    barrier = pltpu.get_barrier_semaphore()
    expected = 0
    for size, stride in dims:
        position = (me // stride) % size
        for step, ok in ((1, position + 1 < size), (-1, position > 0)):
            def signal(step=step, stride=stride):
                pl.semaphore_signal(
                    barrier, inc=1, device_id={"fs": me + step * stride}, device_id_type=MESH
                )

            pl.when(ok)(signal)
            expected = expected + jnp.where(ok, 1, 0)
    pl.semaphore_wait(barrier, expected)

    main, mix = gather_plan(dims, refs, outs, blocks)
    number_sends(main)
    number_sends(mix)
    deepest = sum(size - 1 for size, _ in dims) + 1
    early = min(3, deepest)

    locals_ = []
    for i, (ref, out) in enumerate(zip(refs, outs)):
        if beside is not None and i in (2, 4):
            continue
        locals_.append(pltpu.make_async_copy(ref, out.at[me], local_sem.at[i]))

    go = functools.partial(spread, send_sem=send_sem, recv_sem=recv_sem)
    def shard_in(source, stage, sem, shard, across):
        return pltpu.make_async_copy(
            source, stage.at[:, pl.ds(shard * across, across)], sem.at[shard]
        )

    def lay_in(own, part, stage, sem, rows, height):
        for shard in range(part.shape[0]):
            for mine, source in ((True, own), (False, part.at[shard])):

                @pl.when((me == shard) if mine else (me != shard))
                def _(source=source, shard=shard):
                    piece = source.at[pl.ds(rows, height), :]
                    shard_in(piece, stage, sem, shard, part.shape[2]).start()

    def lay_out(part, whole, stage, sem, rows, height, mode):
        if mode == "start":
            for shard in range(part.shape[0]):
                piece = part.at[shard, pl.ds(rows, height), :]
                shard_in(piece, stage, sem, shard, part.shape[2]).wait()
        copy = pltpu.make_async_copy(
            stage, whole.at[pl.ds(rows, height), :], sem.at[part.shape[0]]
        )
        copy.start() if mode == "start" else copy.wait()

    if beside is not None:
        down_stage, mix_stage, down_sem, mix_sem = args[13:]
        tall = down_stage.shape[1]

        pooled = mix_stage.shape[0]

    def rows_of(c):
        return c * tall if isinstance(c, int) else pl.multiple_of(c * tall, 16)

    def down_in(c):
        slot = c % 2
        lay_in(refs[2], outs[2], down_stage.at[slot], down_sem.at[slot], rows_of(c), tall)

    def down_out(c, mode="start"):
        slot = c % 2
        lay_out(outs[2], beside[0], down_stage.at[slot], down_sem.at[slot], rows_of(c), tall, mode)

    go(mix, me, blocks, low=0, high=1, mode="start")
    go(main, me, 0, low=0, high=1, mode="start")
    for copy in locals_:
        copy.start()
    go(mix, me, blocks, low=1, high=deepest, mode="start")
    if beside is not None:
        lay_in(refs[4], outs[4], mix_stage, mix_sem, 0, pooled)

    def step(i, carry):
        @pl.when(i + 1 < blocks)
        def _():
            go(main, me, i + 1, low=0, high=1, mode="start")

        go(main, me, i, low=1, high=early, mode="start")

        @pl.when(i > 0)
        def _():
            go(main, me, i - 1, low=early, high=deepest, mode="start")

        if beside is not None:

            @pl.when(i > 2)
            def _():
                down_out(i - 3, "end")

            @pl.when(i > 0)
            def _():
                down_in(i - 1)

            @pl.when(i > 1)
            def _():
                down_out(i - 2)

        return carry

    lax.fori_loop(0, blocks, step, 0)
    go(main, me, blocks - 1, low=early, high=deepest, mode="start")
    if beside is not None:
        if blocks > 2:
            down_out(blocks - 3, "end")
        down_in(blocks - 1)
        if blocks > 1:
            down_out(blocks - 2)
        lay_out(outs[4], beside[1], mix_stage, mix_sem, 0, pooled, "start")
        down_out(blocks - 1)

    def finish(i, carry):
        go(main, me, i, low=0, high=deepest, mode="end")
        return carry

    lax.fori_loop(0, blocks, finish, 0)
    go(mix, me, blocks, low=0, high=deepest, mode="end")
    if beside is not None:
        if blocks > 1:
            down_out(blocks - 2, "end")
        down_out(blocks - 1, "end")
        lay_out(outs[4], beside[1], mix_stage, mix_sem, 0, pooled, "end")
    for copy in locals_:
        copy.wait()


def gather_weights(dims, w_gate, w_up, w_down, w_mix_in, w_mix_out):
    count = 1
    for size, _ in dims:
        count *= size
    tiles = (w_gate.shape[0] // 16, w_down.shape[0] // 16)
    blocks = next(b for b in (8, 4, 2, 1) if tiles[0] % b == 0 and tiles[1] % b == 0)
    weights = (w_gate, w_up, w_down, w_mix_in, w_mix_out)
    shapes = [jax.ShapeDtypeStruct((count, *a.shape), a.dtype) for a in weights]

    class Shape:
        def __init__(self, shape):
            self.shape = shape

    stand_in = [Shape(a.shape) for a in weights]
    main, mix = gather_plan(dims, stand_in, [Shape(s.shape) for s in shapes], blocks)
    sends = max(number_sends(main), number_sends(mix))
    scratch = [
        pltpu.SemaphoreType.DMA((blocks + 1, sends)),
        pltpu.SemaphoreType.DMA((blocks + 1, len(main), count)),
        pltpu.SemaphoreType.DMA((5,)),
    ]
    laid = w_down.shape[1] % 128 == 0
    if laid:
        tall, full = w_down.shape[0] // blocks, w_down.shape[1] * count
        shapes += [jax.ShapeDtypeStruct((a.shape[0], full), a.dtype) for a in (w_down, w_mix_out)]
        scratch += [
            pltpu.VMEM((2, tall, full), w_down.dtype),
            pltpu.VMEM((w_mix_out.shape[0], full), w_mix_out.dtype),
            pltpu.SemaphoreType.DMA((2, count + 1)),
            pltpu.SemaphoreType.DMA((count + 1,)),
        ]
    outs = pl.pallas_call(
        functools.partial(gather_kernel, dims, blocks),
        out_shape=shapes,
        in_specs=[pl.BlockSpec(memory_space=pltpu.HBM)] * 5,
        out_specs=[pl.BlockSpec(memory_space=pltpu.HBM)] * len(shapes),
        scratch_shapes=scratch,
        compiler_params=pltpu.CompilerParams(collective_id=0, has_side_effects=True),
        name="gather_weights",
    )(*weights)

    def stacked(a):
        return a.reshape(-1, a.shape[2])

    def beside(a):
        return jnp.transpose(a, (1, 0, 2)).reshape(a.shape[1], -1)

    gate, up, down, mix_in, mix_out = outs[:5]
    if laid:
        return stacked(gate), stacked(up), outs[5], stacked(mix_in), outs[6]
    return stacked(gate), stacked(up), beside(down), stacked(mix_in), beside(mix_out)


def rms_scale(values, gain):
    return values * lax.rsqrt(jnp.mean(values * values, axis=-1, keepdims=True) + 1e-06) * gain


def total_over_tp(left_rows, right_matrix):
    part = jnp.dot(left_rows, right_matrix, preferred_element_type=jnp.float32)
    part = part.astype(jnp.bfloat16)
    if lax.axis_size("tp") == 2:
        other = lax.ppermute(part, "tp", ((0, 1), (1, 0)))
        return part.astype(jnp.float32) + other.astype(jnp.float32)
    return lax.psum(part.astype(jnp.float32), "tp")


def own_total_over_tp(left_rows, right_matrix):
    part = jnp.dot(left_rows, right_matrix, preferred_element_type=jnp.float32)
    part = part.astype(jnp.bfloat16)
    if lax.axis_size("tp") == 2:
        mine = own_rows_of(part)
        half = mine.shape[0]
        theirs = lax.dynamic_slice_in_dim(part, (1 - lax.axis_index("tp")) * half, half, 0)
        other = lax.ppermute(theirs, "tp", ((0, 1), (1, 0)))
        return mine.astype(jnp.float32) + other.astype(jnp.float32)
    return lax.psum_scatter(part.astype(jnp.float32), "tp", scatter_dimension=0, tiled=True)


def own_rows_of(array):
    count = array.shape[0] // lax.axis_size("tp")
    return lax.dynamic_slice_in_dim(array, lax.axis_index("tp") * count, count, 0)


def body(dims, tokens, w_gate, w_up, w_down, w_mix_in, w_mix_out, pool_w, pool_scale, norm_gains):
    rows_all = tokens.shape[0]
    stream = tokens.astype(jnp.float32)
    normed = rms_scale(stream, norm_gains[0]).astype(jnp.bfloat16)
    gate_full, up_full, down_full, mix_in_full, mix_out_full = gather_weights(
        dims, w_gate, w_up, w_down, w_mix_in, w_mix_out
    )
    gate_first = jnp.dot(normed, gate_full, preferred_element_type=jnp.float32)
    up_first = jnp.dot(normed, up_full, preferred_element_type=jnp.float32)
    hidden = (jax.nn.silu(gate_first) * up_first).astype(jnp.bfloat16)
    stream = stream + 0.5 * rms_scale(total_over_tp(hidden, down_full), norm_gains[1])
    normed = rms_scale(stream, norm_gains[2]).astype(jnp.bfloat16)
    pooled_in = jnp.dot(normed, mix_in_full, preferred_element_type=jnp.float32)
    pooled_in = pooled_in.astype(jnp.bfloat16)
    groups_here = pool_w.shape[0]
    group_dim = pool_w.shape[1]
    values = pooled_in.astype(jnp.float32).reshape(rows_all // LEN, LEN, groups_here, group_dim)
    totals = jnp.cumsum(values, axis=1)
    position = jnp.arange(1, LEN + 1).astype(jnp.float32)[None, :, None, None]
    window_ids = (lax.axis_index("tp") * groups_here + jnp.arange(groups_here)) % 4
    average = jnp.zeros_like(values)
    for window_slot in range(4):
        window = 2 ** (1 + window_slot)
        lagged = jnp.pad(totals, ((0, 0), (window, 0), (0, 0), (0, 0)))[:, :LEN]
        candidate = (totals - lagged) / jnp.minimum(position, float(window))
        average = jnp.where((window_ids == window_slot)[None, None, :, None], candidate, average)
    deviation = (average - values).astype(jnp.bfloat16)
    regrouped = jnp.einsum("btgi,gio->btgo", deviation, pool_w, preferred_element_type=jnp.float32)
    regrouped = (
        regrouped.reshape(rows_all, groups_here * group_dim) * pool_scale.astype(jnp.float32)
    ).astype(jnp.bfloat16)
    stream = stream + rms_scale(total_over_tp(regrouped, mix_out_full), norm_gains[3])
    normed = rms_scale(stream, norm_gains[4]).astype(jnp.bfloat16)
    gate_second = jnp.dot(normed, gate_full, preferred_element_type=jnp.float32)
    up_second = jnp.dot(normed, up_full, preferred_element_type=jnp.float32)
    hidden = (jax.nn.silu(gate_second) * up_second).astype(jnp.bfloat16)
    stream_own = own_rows_of(stream)
    stream_own = stream_own + 0.5 * rms_scale(own_total_over_tp(hidden, down_full), norm_gains[5])
    return stream_own.astype(jnp.bfloat16)


def solution(mesh):
    in_specs = (
        P("fs", None),
        P("fs", "tp"),
        P("fs", "tp"),
        P("tp", "fs"),
        P("fs", "tp"),
        P("tp", "fs"),
        P("tp", None, None),
        P("tp"),
        P(),
    )
    out_specs = P(("fs", "tp"), None)
    return jax.shard_map(functools.partial(body, line_dims(mesh)), mesh=mesh, in_specs=in_specs, out_specs=out_specs, check_vma=False)
```

profile of v0, /device:TPU:0, one launch (start us, length us, event | category | flops | bytes accessed | tf_op | source)
XLA Modules:
  0.0 390.9 jit_solution(15200503720500681430)
XLA Ops:
  0.0 0.0 copy-start
  0.0 0.0 copy-start.2
  0.0 1.2 fusion.30
  1.2 1.7 fusion.2
  2.8 300.4 %gather_weights.1 = (bf16[16,128,2816]{2,1,0:T(8,128)(2,1)}, bf16[16,128,2816]{2,1,0:T(8,128)(2,1)}, bf16[16,2816,128]{2,1,0:T(8,128)(2,1)}, bf16[16,128,512]{2,...) custom-call(bf16[128,2816]{1,0:T(8,128)(2,1)} %args_0_.4, ...), custom_call_target="tpu_custom_call" | custom-call | tf_op jit(solution)/shard_map/gather_weights/pallas_call | solution.py:351
  303.2 0.0 copy-done.2
  303.2 8.8 %fusion.20 = f32[320,2816]{1,0:T(8,128)} fusion(bf16[2048,2816]{1,0:T(8,128)(2,1)} %bitcast.45, bf16[320,2048]{1,0:T(8,128)(2,1)S(1)} %copy-done.2, f32[2048]{0:T(1024)S(1)} %bitcast.41, f32[320]{0:T(512)S(1)} %add_rsqrt_fusion.4), kind=kOutput, calls=%fused_computation.47 | convolution fusion | flops 3693608960 | bytes 16459008 | tf_op jit(solution)/shard_map/dot_general | solution.py:410
  312.0 0.0 copy-start.5
  312.0 16.4 %convolution_convert_fusion.2 = bf16[320,2048]{1,0:T(8,128)(2,1)S(1)} fusion(bf16[2816,2048]{1,0:T(8,128)(2,1)} %get-tuple-element.12, bf16[2048,2816]{1,0:T(8,128)(2,1)} %bitcast.43, f32[320,2816]{1,0:T(8,128)} %fusion.20, bf16[320,2048]{1,0:T(8,128)(2,1)S(1)} %copy-done.2, f32[2048]{0:T(1024)S(1)} %bitcast.42, f32[320]{0:T(512)S(1)} %add_rsqrt_fusion.4), kind=kOutput, calls=%fused_computation.9 | convolution fusion | flops 7390658560 | bytes 29304064 | tf_op jit(solution)/shard_map/dot_general | solution.py:378
  328.4 0.1 collective-permute-start
  328.5 0.0 copy-done.5
  328.6 3.1 collective-permute-done
  331.6 1.8 multiply_reduce_fusion.3
  333.5 0.0 copy-start.7
  333.5 2.4 multiply_reduce_fusion.2
  335.9 0.0 copy-done.7
  335.9 3.3 fusion.9
  339.3 1.3 reshape.118
  340.6 0.0 copy-start.6
  340.6 0.1 fusion.31
  340.7 1.8 fusion.17
  342.5 0.0 copy-done
  342.5 0.2 convolution_bitcast_fusion
  342.8 0.4 copy.12
  343.2 0.0 copy-done.6
  343.2 1.9 convolution_convert_fusion
  345.1 0.1 collective-permute-start.1
  345.3 3.2 collective-permute-done.1
  348.5 2.2 multiply_reduce_fusion.1
  350.8 3.6 multiply_reduce_fusion
  354.4 0.0 copy-start.3
  354.4 1.5 copy-done.3
  355.9 8.7 %fusion.29 = f32[320,2816]{1,0:T(8,128)} fusion(bf16[2048,2816]{1,0:T(8,128)(2,1)} %bitcast.46, f32[320,2048]{1,0:T(8,128)S(1)} %get-tuple-element.16, f32[2048]{0:T(1024)S(1)} %bitcast.38, f32[320]{0:T(512)S(1)} %add_rsqrt_fusion), kind=kOutput, calls=%fused_computation.73 | convolution fusion | flops 3692953600 | bytes 17769728 | tf_op jit(solution)/shard_map/dot_general | solution.py:436
  364.6 18.2 %convolution_convert_fusion.1 = bf16[320,2048]{1,0:T(8,128)(2,1)} fusion(bf16[2816,2048]{1,0:T(8,128)(2,1)} %get-tuple-element.12, bf16[2048,2816]{1,0:T(8,128)(2,1)} %bitcast.44, f32[320,2816]{1,0:T(8,128)} %fusion.29, f32[320,2048]{1,0:T(8,128)} %copy-done.3, f32[2048]{0:T(1024)S(1)} %bitcast.39, f32[320]{0:T(512)S(1)} %add_rsqrt_fusion), kind=kOutput, calls=%fused_computation.8 | convolution fusion | flops 7390003200 | bytes 30614784 | tf_op jit(solution)/shard_map/dot_general | solution.py:387
  382.7 0.0 copy-start.4
  382.7 0.0 copy-start.1
  382.8 2.1 constant_dynamic-slice_fusion
  384.9 0.1 collective-permute-start.2
  385.0 2.2 collective-permute-done.2
  387.2 1.4 multiply_reduce_fusion.4
  388.6 0.0 copy-done.4
  388.6 2.3 add_convert_fusion
  390.9 0.0 copy-done.1
  (11 shorter events, 0.1 us)
Async XLA Ops:
  0.0 342.5 %copy-start = (bf16[4,128,128]{2,1,0:T(8,128)(2,1)S(1)}, bf16[4,128,128]{2,1,0:T(8,128)(2,1)}, u32[]{:S(2)}) copy-start(bf16[4,128,128]{2,1,0:T(8,128)(2,1)} %param.15) | copy-start | bytes 393220
  0.0 303.2 %copy-start.2 = (bf16[320,2048]{1,0:T(8,128)(2,1)S(1)}, bf16[320,2048]{1,0:T(8,128)(2,1)}, u32[]{:S(2)}) copy-start(bf16[320,2048]{1,0:T(8,128)(2,1)} %param.9) | copy-start | bytes 3932164
  312.0 16.5 %copy-start.5 = (bf16[512]{0:T(512)(128)(2,1)S(1)}, bf16[512]{0:T(512)(128)(2,1)}, u32[]{:S(2)}) copy-start(bf16[512]{0:T(512)(128)(2,1)} %param.16) | copy-start | bytes 3076
  328.4 3.2 collective-permute-start
  333.5 2.5 copy-start.7
  340.6 2.6 copy-start.6
  345.1 3.4 collective-permute-start.1
  354.4 1.5 copy-start.3
  382.7 5.8 %copy-start.4 = (f32[320,2048]{1,0:T(8,128)S(1)}, f32[320,2048]{1,0:T(8,128)}, u32[]{:S(2)}) copy-start(f32[320,2048]{1,0:T(8,128)} %copy-done.3) | copy-start | bytes 7864324
  382.7 8.2 %copy-start.1 = (bf16[4,128,128]{2,1,0:T(8,128)(2,1)S(1)}, bf16[4,128,128]{2,1,0:T(8,128)(2,1)}, u32[]{:S(2)}) copy-start(bf16[4,128,128]{2,1,0:T(8,128)(2,1)} %param.15) | copy-start | bytes 393220
  384.9 2.3 collective-permute-start.2
where the time goes:
time: 391 us
  Pallas kernels  300 us (77%)
  matrix products  57.6 us (15%)
  other arithmetic  17.5 us (4%)
  waiting for transfers between devices  8.47 us (2%)
  local copies, waits for them, and re-layouts  6.51 us (2%)
    pallas_call x1, Pallas kernels, gather_weights(): pl.pallas_call(functools.partial(gather_kernel, dims, blocks), out_shape=...  300 us
    dot_general x2, matrix products, total_over_tp(): part = jnp.dot(left_rows, right_matrix, preferred_element_type=jnp.float32)  18.3 us
    dot_general x1, matrix products, own_total_over_tp(): part = jnp.dot(left_rows, right_matrix, preferred_element_type=jnp.float32)  18.2 us
    reduce_sum x6, other arithmetic, rms_scale(): jnp.mean(values * values, axis=-1, keepdims=True) + 1e-06  13.2 us
    dot_general x1, matrix products, body(): gate_first = jnp.dot(normed, gate_full, preferred_element_type=jnp.float32)  8.75 us
    dot_general x1, matrix products, body(): gate_second = jnp.dot(normed, gate_full, preferred_element_type=jnp.float32)  8.72 us
  transfers between devices with their start and end apart: 3, of which 3 were waited for; matrix products, arithmetic and copies ran while one was open for 0% of the time, Pallas kernels for 0%

commit v1 on v0

--- a/solution.py
+++ b/solution.py
@@ -441,6 +441,526 @@
     return stream_own.astype(jnp.bfloat16)
 
 
+def silu(v):
+    return v / (1.0 + jnp.exp(-v))
+
+
+def rms_value(values, gain):
+    return values * lax.rsqrt(jnp.mean(values * values, axis=-1, keepdims=True) + 1e-06) * gain
+
+
+class Sends:
+    def __init__(self, sem):
+        self.sem, self.count, self.pending = sem, 0, []
+
+    def put(self, src, dst, recv, to, ok=None):
+        copy = pltpu.make_async_remote_copy(
+            src_ref=src,
+            dst_ref=dst,
+            send_sem=self.sem.at[self.count],
+            recv_sem=recv,
+            device_id=to,
+            device_id_type=MESH,
+        )
+        self.count += 1
+        when(ok, copy.start)
+        self.pending.append((ok, copy))
+
+    def drain(self):
+        for ok, copy in self.pending:
+            when(ok, copy.wait_send)
+        self.pending = []
+
+
+SENDS = 192
+F32, BF16 = jnp.float32, jnp.bfloat16
+
+
+def layer_kernel(dims, *refs):
+    (tokens, gate, up, down, mix_in, mix_out, pool_w, pool_scale, gains, out) = refs[:10]
+    (gate_v, up_v, down_v, min_v, mout_v) = refs[10:15]
+    (tok_v, norm_v, own_v, far_v, hid_v, part_v, part2_v, partm_v) = refs[15:23]
+    (got1, got2o, got2f, gotm, sum1, sum2, far1, far2) = refs[23:31]
+    (stream_v, mid_v, pin_v, rg_v, out_v) = refs[31:36]
+    (send_sem, ff_sem, mix_sem, act_sem, local_sem, loc_ff) = refs[36:]
+    (nz, sz), (_, sy), (_, sx) = dims
+    me, core = lax.axis_index("fs"), lax.axis_index("tp")
+    z = me // sz
+    col = me - z * sz
+    xn = me + (1 - 2 * ((me // sx) % 2)) * sx
+    yn = me + (1 - 2 * ((me // sy) % 2)) * sy
+    dg = xn + yn - me
+    sign = 1 - 2 * (z % 2)
+    peer = me + sign * sz
+    depth = gate.shape[0]
+    hid = gate_v.shape[1]
+    rows = tokens.shape[0]
+    half = rows // 2
+    wide = down.shape[1]
+    feat = tokens.shape[1]
+    span = sz * wide
+
+    barrier = pltpu.get_barrier_semaphore()
+    friends = [({"fs": xn}), ({"fs": yn}), ({"tp": 1 - core})]
+    for k in range(1, nz):
+        friends.append({"fs": lax.rem(z + k, nz) * sz + col})
+    for to in friends:
+        pl.semaphore_signal(barrier, inc=1, device_id=to, device_id_type=MESH)
+    pl.semaphore_wait(barrier, len(friends))
+
+    sends = Sends(send_sem)
+
+    def mo(v, n):
+        return v if isinstance(v, int) else pl.multiple_of(v, n)
+
+    def plane(p):
+        return near(z, nz, p)[0] if p else z
+
+    weights = ((gate, gate_v), (up, up_v), (down, down_v))
+
+    def own_piece(m, h, u):
+        ref = weights[m][0]
+        if m < 2:
+            return ref.at[pl.ds(u * (depth // 2), depth // 2), pl.ds(mo(h * hid, 128), hid)]
+        return ref.at[pl.ds(mo(h * hid + u * (hid // 2), 16), hid // 2), :]
+
+    def place(m, src, u):
+        buf = weights[m][1]
+        if m < 2:
+            return buf.at[pl.ds(mo(src * depth + u * (depth // 2), 16), depth // 2), :]
+        return buf.at[src, pl.ds(u * (hid // 2), hid // 2), :]
+
+    def arrived(ref, sem):
+        pltpu.make_async_copy(ref, ref, sem).wait()
+
+    locals_ = {}
+
+    def local(key, src, dst, sem):
+        copy = pltpu.make_async_copy(src, dst, sem)
+        copy.start()
+        locals_[key] = copy
+
+    steps = [(m, p) for m in range(4) for p in range(nz)]
+
+    def pieces(m):
+        return range(2) if m < 3 else range(1)
+
+    def spot(m, src, u):
+        return place(m, src, u) if m < 3 else mout_v.at[src]
+
+    def sem_of(m, src, u):
+        return ff_sem.at[m, src, u]
+
+    def origin(m, h, u):
+        return own_piece(m, h, u) if m < 3 else mix_out
+
+    def stage0(n):
+        m, p = steps[n]
+        if p == 0:
+            return
+        t = plane(p)
+        for u in pieces(m):
+            sends.put(origin(m, t % 2, u), spot(m, me, u), sem_of(m, me, u), {"fs": t * sz + col})
+
+    def stage1(n):
+        m, p = steps[n]
+        src = plane(p) * sz + col
+        for u in pieces(m):
+            if p:
+                arrived(spot(m, src, u), sem_of(m, src, u))
+            for nb in (xn, yn):
+                first = spot(m, src, u) if p else origin(m, z % 2, u)
+                sends.put(first, spot(m, src, u), sem_of(m, src, u), {"fs": nb})
+            if not p:
+                local((m, u), origin(m, z % 2, u), spot(m, me, u), loc_ff.at[m, u])
+
+    def three(p):
+        shift = plane(p) * sz - z * sz
+        return xn + shift, yn + shift, dg + shift
+
+    def relay(m, p, u, across):
+        a, b, _ = three(p)
+        src, to = (a, yn) if across else (b, xn)
+        arrived(spot(m, src, u), sem_of(m, src, u))
+        sends.put(spot(m, src, u), spot(m, src, u), sem_of(m, src, u), {"fs": to})
+
+    def stage2(n):
+        m, p = steps[n]
+        if m < 3:
+            relay(m, p, 0, True)
+            relay(m, p, 1, False)
+        else:
+            relay(m, p, 0, p % 2 == 0)
+
+    def stage3(n):
+        m, p = steps[n]
+        a, b, d = three(p)
+        if m < 3:
+            todo = [(a, 1), (b, 0), (d, 0), (d, 1)]
+        else:
+            todo = [(b if p % 2 == 0 else a, 0), (d, 0)]
+        for src, u in todo:
+            arrived(spot(m, src, u), sem_of(m, src, u))
+        if p == 0:
+            for u in pieces(m):
+                locals_[(m, u)].wait()
+
+    def min_at(src):
+        return min_v.at[pl.ds(mo(src * depth, 16), depth), :]
+
+    def mix_own():
+        for nb in (xn, yn):
+            sends.put(mix_in, min_at(me), mix_sem.at[me], {"fs": nb})
+        local("mix", mix_in, min_at(me), local_sem.at[0])
+
+    def mix_turn():
+        arrived(min_at(xn), mix_sem.at[xn])
+        sends.put(min_at(xn), min_at(xn), mix_sem.at[xn], {"fs": yn})
+
+    def mix_up():
+        arrived(min_at(yn), mix_sem.at[yn])
+        arrived(min_at(dg), mix_sem.at[dg])
+        locals_["mix"].wait()
+        for src in (me, xn, yn, dg):
+            for step in (1, -1):
+                ok = jnp.logical_and(z + step >= 0, z + step < nz)
+                sends.put(min_at(src), min_at(src), mix_sem.at[src], {"fs": me + step * sz}, ok)
+
+    def mix_on(p, forward=True):
+        found, away = near(z, nz, p)
+        shift = (found - z) * sz
+        inside = jnp.logical_and(z + away >= 0, z + away < nz)
+        for src in (me + shift, xn + shift, yn + shift, dg + shift):
+            here, sem = min_at(src), mix_sem.at[src]
+            if forward:
+                when(inside, functools.partial(arrived, here, sem))
+                sends.put(here, here, sem, {"fs": me + away * sz}, inside)
+            else:
+                when(jnp.logical_not(inside), functools.partial(arrived, here, sem))
+
+    mine = pl.ds(mo(core * half, 16), half)
+    theirs = pl.ds(mo((1 - core) * half, 16), half)
+    mine_far = pl.ds(mo(rows + core * half, 16), half)
+    theirs_far = pl.ds(mo(rows + (1 - core) * half, 16), half)
+    partner = {"tp": 1 - core}
+    buddy = {"fs": peer}
+
+    def tokens_out():
+        sends.put(tokens.at[mine, :], tok_v.at[mine_far, :], act_sem.at[0], buddy)
+        local("tok", tokens, tok_v.at[pl.ds(0, rows), :], local_sem.at[1])
+
+    def tokens_on():
+        here = tok_v.at[mine_far, :]
+        arrived(here, act_sem.at[0])
+        sends.put(here, here, act_sem.at[1], partner)
+
+    def first_norm():
+        arrived(tok_v.at[theirs_far, :], act_sem.at[1])
+        locals_["tok"].wait()
+
+        def block(i, carry):
+            at = pl.ds(pl.multiple_of(i * 32, 32), 32)
+            v = tok_v[at, :].astype(F32)
+            norm_v[at, :] = rms_value(v, gains[0:1, :]).astype(BF16)
+            return carry
+
+        lax.fori_loop(0, 2 * rows // 32, block, 0)
+
+    def gate_up(src, at, dst):
+        def tile(cols, n):
+            w = jnp.concatenate([gate_v[:, cols], up_v[:, cols]], axis=1)
+            both = jnp.dot(src[at, :], w, preferred_element_type=F32)
+            hid_v[dst, cols] = (silu(both[:, :n]) * both[:, n:]).astype(BF16)
+
+        whole = hid // 256
+
+        def body(j, carry):
+            tile(pl.ds(pl.multiple_of(j * 256, 256), 256), 256)
+            return carry
+
+        lax.fori_loop(0, whole, body, 0)
+        if hid % 256:
+            tile(pl.ds(whole * 256, hid % 256), hid % 256)
+
+    def down_block(t, at):
+        w = jnp.concatenate([down_v[t * sz + i] for i in range(sz)], axis=1)
+        return jnp.dot(hid_v[at, :], w, preferred_element_type=F32).astype(BF16)
+
+    def cols_of(t):
+        return pl.ds(mo(t * span, 128), span)
+
+    def down1(p):
+        t = plane(p)
+        cols = cols_of(t)
+        for i, (base, other) in enumerate(((rows, theirs_far), (0, theirs))):
+            at = pl.ds(base, rows)
+            part_v[at, cols] = down_block(t, at)
+            sends.put(part_v.at[other, cols], got1.at[1 - i, :, cols], act_sem.at[8 + 2 * p + i], partner)
+
+    def reduce1(p):
+        cols = cols_of(plane(p))
+        for i in range(2):
+            arrived(got1.at[1 - i, :, cols], act_sem.at[8 + 2 * p + i])
+        total = part_v[mine_far, cols].astype(F32) + got1[1, :, cols].astype(F32)
+        sum1[:, cols] = total.astype(BF16)
+        sends.put(sum1.at[:, cols], far1.at[:, cols], act_sem.at[16 + plane(p)], buddy)
+
+    def first_stream():
+        for t in range(nz):
+            cols = cols_of(t)
+            arrived(far1.at[:, cols], act_sem.at[16 + t])
+
+        def block(i, carry):
+            r = pl.ds(pl.multiple_of(i * 16, 16), 16)
+            at = pl.ds(pl.multiple_of(core * half + i * 16, 16), 16)
+            y = part_v[at, :].astype(F32) + got1[0, r, :].astype(F32) + far1[r, :].astype(F32)
+            s = tok_v[at, :].astype(F32) + 0.5 * rms_value(y, gains[1:2, :])
+            stream_v[r, :] = s
+            mid_v[at, :] = rms_value(s, gains[2:3, :]).astype(BF16)
+            return carry
+
+        lax.fori_loop(0, half // 16, block, 0)
+        sends.put(mid_v.at[mine, :], mid_v.at[mine, :], act_sem.at[2], partner)
+
+    def into_pool(at):
+        v = jnp.dot(mid_v[at, :], min_v[...], preferred_element_type=F32)
+        pin_v[at, :] = v.astype(BF16).astype(F32)
+
+    def pool():
+        length = LEN
+        groups, dim = pool_w.shape[0], pool_w.shape[1]
+        t = lax.broadcasted_iota(jnp.int32, (rows, dim), 0) % length
+        for g in range(groups):
+            cols = slice(g * dim, (g + 1) * dim)
+            v = pin_v[:, cols]
+            window = 2 ** (1 + g % 4)
+            total, k = v, 1
+            while k < window:
+                total = total + jnp.where(t >= k, pltpu.roll(total, k, 0), 0.0)
+                k *= 2
+            count = jnp.minimum(t + 1, window).astype(F32)
+            dev = (total / count - v).astype(BF16)
+            o = jnp.dot(dev, pool_w[g], preferred_element_type=F32) * pool_scale[:, cols]
+            rg_v[:, cols] = o.astype(BF16)
+
+    def out_pool(at):
+        for t in range(nz):
+            w = jnp.concatenate([mout_v[t * sz + i] for i in range(sz)], axis=1)
+            v = jnp.dot(rg_v[at, :], w, preferred_element_type=F32)
+            partm_v[at, pl.ds(t * span, span)] = v.astype(BF16)
+
+    quarter = half // 2
+
+    def second_stream():
+        arrived(gotm, act_sem.at[3])
+
+        def block(i, carry):
+            r = pl.ds(pl.multiple_of(i * 16, 16), 16)
+            at = pl.ds(pl.multiple_of(core * half + i * 16, 16), 16)
+            y = partm_v[at, :].astype(F32) + gotm[r, :].astype(F32)
+            s = stream_v[r, :] + rms_value(y, gains[3:4, :])
+            stream_v[r, :] = s
+            own_v[at, :] = rms_value(s, gains[4:5, :]).astype(BF16)
+            return carry
+
+        for k in range(2):
+            lax.fori_loop(k * quarter // 16, (k + 1) * quarter // 16, block, 0)
+            src = own_v.at[pl.ds(mo(core * half + k * quarter, 16), quarter), :]
+            sends.put(src, far_at(k, core), act_sem.at[4 + k], buddy)
+        sends.put(own_v.at[mine, :], own_v.at[mine, :], act_sem.at[6], partner)
+
+    def far_at(k, c):
+        return far_v.at[pl.ds(mo((2 * k + c) * quarter, 16), quarter), :]
+
+    def far_on(k):
+        arrived(far_at(k, core), act_sem.at[4 + k])
+        sends.put(far_at(k, core), far_at(k, core), act_sem.at[20 + k], partner)
+
+    def down2(dst, base, count):
+        at = pl.ds(base, count)
+
+        def body(t, carry):
+            part2_v[at, pl.ds(pl.multiple_of(t * span, 128), span)] = down_block(t, at)
+            return carry
+
+        lax.fori_loop(0, nz, body, 0)
+
+    def far_part(k, c):
+        return pl.ds(mo(rows + (2 * k + c) * quarter, 16), quarter)
+
+    last = len(steps)
+    stage1(0)
+    for n in (1, 2, 3):
+        stage0(n)
+    mix_own()
+    tokens_out()
+    stage0(5)
+    stage1(1)
+    stage2(0)
+    mix_turn()
+    all_mine = pl.ds(0, rows)
+    all_far = pl.ds(rows, rows)
+
+    def advance(i):
+        if i + 6 < last:
+            stage0(i + 6)
+        if i + 2 < last:
+            stage1(i + 2)
+        if i + 1 < last:
+            stage2(i + 1)
+        stage3(i)
+
+    for i in range(3 * nz):
+        advance(i)
+        if i == 2:
+            tokens_on()
+        if i == 4:
+            first_norm()
+        if i == nz + 1:
+            mix_up()
+        if i == 2 * nz - 1:
+            gate_up(norm_v, all_mine, all_mine)
+        if i == 2 * nz:
+            gate_up(norm_v, all_far, all_far)
+        if i == 2 * nz + 1:
+            down1(0)
+            down1(1)
+            mix_on(1)
+        if 2 * nz + 1 < i:
+            down1(i - 2 * nz)
+            if i == 2 * nz + 2:
+                reduce1(0)
+                mix_on(2)
+            reduce1(i - 2 * nz - 1)
+    for p in range(3, nz):
+        mix_on(p)
+    advance(3 * nz)
+    reduce1(nz - 1)
+    for i in range(3 * nz + 1, last - 1):
+        advance(i)
+    first_stream()
+    for p in range(1, nz):
+        mix_on(p, forward=False)
+    into_pool(mine)
+    arrived(mid_v.at[theirs, :], act_sem.at[2])
+    into_pool(theirs)
+    pool()
+    advance(last - 1)
+    out_pool(theirs)
+    sends.put(partm_v.at[theirs, :], gotm, act_sem.at[3], partner)
+    out_pool(mine)
+    second_stream()
+
+    arrived(own_v.at[theirs, :], act_sem.at[6])
+    gate_up(own_v, all_mine, all_mine)
+    down2(own_v, 0, rows)
+    sends.put(part2_v.at[theirs, :], got2o, act_sem.at[7], partner)
+    for k in range(2):
+        far_on(k)
+        arrived(far_at(k, 1 - core), act_sem.at[20 + k])
+        base = 2 * k * quarter
+        gate_up(far_v, pl.ds(base, 2 * quarter), pl.ds(rows + base, 2 * quarter))
+        down2(far_v, rows + base, 2 * quarter)
+        sends.put(part2_v.at[far_part(k, 1 - core), :], got2f.at[k], act_sem.at[22 + k], partner)
+        arrived(got2f.at[k], act_sem.at[22 + k])
+        total = part2_v[far_part(k, core), :].astype(F32) + got2f[k].astype(F32)
+        sum2[k] = total.astype(BF16)
+        there = far2.at[pl.ds(k * quarter, quarter), :]
+        sends.put(sum2.at[k], there, act_sem.at[24 + k], buddy)
+    arrived(got2o, act_sem.at[7])
+
+    def last_block(i, carry):
+        r = pl.ds(pl.multiple_of(i * 16, 16), 16)
+        at = pl.ds(pl.multiple_of(core * half + i * 16, 16), 16)
+        y = part2_v[at, :].astype(F32) + got2o[r, :].astype(F32) + far2[r, :].astype(F32)
+        s = stream_v[r, :] + 0.5 * rms_value(y, gains[5:6, :])
+        out_v[r, :] = s.astype(BF16)
+        return carry
+
+    for k in range(2):
+        arrived(far2.at[pl.ds(k * quarter, quarter), :], act_sem.at[24 + k])
+        lax.fori_loop(k * quarter // 16, (k + 1) * quarter // 16, last_block, 0)
+    final = pltpu.make_async_copy(out_v, out, local_sem.at[2])
+    final.start()
+    sends.drain()
+    final.wait()
+
+
+def whole_layer(dims, tokens, w_gate, w_up, w_down, w_mix_in, w_mix_out, pool_w, pool_scale, gains):
+    count = 1
+    for size, _ in dims:
+        count *= size
+    nz = dims[0][0]
+    depth, units = w_gate.shape
+    hid = units // 2
+    rows, feat = tokens.shape
+    half = rows // 2
+    wide = w_down.shape[1]
+    pooled = w_mix_in.shape[1]
+    scale = pool_scale.astype(F32).reshape(1, -1)
+
+    def buf(*shape, dtype=BF16):
+        return pltpu.VMEM(shape, dtype)
+
+    scratch = [
+        buf(count * depth, hid),
+        buf(count * depth, hid),
+        buf(count, hid, wide),
+        buf(count * depth, pooled),
+        buf(count, w_mix_out.shape[0], wide),
+        buf(2 * rows, feat),
+        buf(2 * rows, feat),
+        buf(rows, feat),
+        buf(rows, feat),
+        buf(2 * rows, hid),
+        buf(2 * rows, feat),
+        buf(2 * rows, feat),
+        buf(rows, feat),
+        buf(2, half, feat),
+        buf(half, feat),
+        buf(2, half // 2, feat),
+        buf(half, feat),
+        buf(half, feat),
+        buf(2, half // 2, feat),
+        buf(half, feat),
+        buf(half, feat),
+        buf(half, feat, dtype=F32),
+        buf(rows, feat),
+        buf(rows, pooled, dtype=F32),
+        buf(rows, pooled),
+        buf(half, feat),
+        pltpu.SemaphoreType.DMA((SENDS,)),
+        pltpu.SemaphoreType.DMA((4, count, 2)),
+        pltpu.SemaphoreType.DMA((count,)),
+        pltpu.SemaphoreType.DMA((32,)),
+        pltpu.SemaphoreType.DMA((4,)),
+        pltpu.SemaphoreType.DMA((4, 2)),
+    ]
+    hbm = pl.BlockSpec(memory_space=pltpu.HBM)
+    vmem = pl.BlockSpec(memory_space=pltpu.VMEM)
+    return pl.pallas_call(
+        functools.partial(layer_kernel, dims),
+        out_shape=jax.ShapeDtypeStruct((half, feat), tokens.dtype),
+        in_specs=[hbm] * 6 + [vmem] * 3,
+        out_specs=hbm,
+        scratch_shapes=scratch,
+        compiler_params=pltpu.CompilerParams(
+            collective_id=1, has_side_effects=True, vmem_limit_bytes=67043328
+        ),
+        name="whole_layer",
+    )(tokens, w_gate, w_up, w_down, w_mix_in, w_mix_out, pool_w, scale, gains)
+
+
+def paired(dims, mesh):
+    return (
+        len(dims) == 3
+        and dims[0][0] == 4
+        and dims[1][0] == 2
+        and dims[2][0] == 2
+        and mesh.shape["tp"] == 2
+    )
+
+
 def solution(mesh):
     in_specs = (
         P("fs", None),
@@ -454,4 +974,8 @@
         P(),
     )
     out_specs = P(("fs", "tp"), None)
-    return jax.shard_map(functools.partial(body, line_dims(mesh)), mesh=mesh, in_specs=in_specs, out_specs=out_specs, check_vma=False)
+    dims = line_dims(mesh)
+    act = whole_layer if paired(dims, mesh) else body
+    return jax.shard_map(
+        functools.partial(act, dims), mesh=mesh, in_specs=in_specs, out_specs=out_specs, check_vma=False
+    )

time: 391 us -> 239 us (0.61)
  the two profiles are of different devices: /device:TPU:0 before, /device:TPU:19 now
where the time goes in v1:
time: 239 us
  Pallas kernels  236 us (99%)
    pallas_call x1, Pallas kernels, whole_layer(): pl.pallas_call(functools.partial(layer_kernel, dims), out_shape=jax.Shape...  236 us

profile of v1, /device:TPU:19, one launch (start us, length us, event | category | flops | bytes accessed | tf_op | source)
XLA Modules:
  0.0 239.3 jit_solution(10315554013378049198)
XLA Ops:
  0.0 1.3 reshape.7
  1.3 236.1 %whole_layer.1 = bf16[160,2048]{1,0:T(8,128)(2,1)} custom-call(bf16[320,2048]{1,0:T(8,128)(2,1)} %refs_0_.1, bf16[128,2816]{1,0:T(8,128)(2,1)} %refs_1_.1, bf16[128,2816]{1,0:T(8,128)(2,1)} %refs_2_.1, bf16[2816,128]{1,0:T(8,128)(2,1)} %refs_3_.1, bf16[128,512]{1,0:T(8,128)(2,1)} %refs_4_.1, bf16[512,128]{1,0:T(8,128)(2,1)} %refs_5_.1, ...), custom_call_target="tpu_custom_call" | custom-call | tf_op jit(solution)/shard_map/whole_layer/pallas_call | solution.py:941
  237.3 2.0 copy.11

commit v2 on v1

--- a/solution.py
+++ b/solution.py
@@ -449,6 +449,15 @@
     return values * lax.rsqrt(jnp.mean(values * values, axis=-1, keepdims=True) + 1e-06) * gain
 
 
+def runs(first, count, most=32):
+    out, at = [], first
+    while at < first + count:
+        size = min(most, first + count - at)
+        out.append((at, size))
+        at += size
+    return out
+
+
 class Sends:
     def __init__(self, sem):
         self.sem, self.count, self.pending = sem, 0, []
@@ -540,7 +549,8 @@
         copy.start()
         locals_[key] = copy
 
-    steps = [(m, p) for m in range(4) for p in range(nz)]
+    steps = [(m, 0) for m in range(2)] + [(m, p) for m in range(2) for p in range(1, nz)]
+    steps += [(m, p) for m in range(2, 4) for p in range(nz)]
 
     def pieces(m):
         return range(2) if m < 3 else range(1)
@@ -710,16 +720,13 @@
             cols = cols_of(t)
             arrived(far1.at[:, cols], act_sem.at[16 + t])
 
-        def block(i, carry):
-            r = pl.ds(pl.multiple_of(i * 16, 16), 16)
-            at = pl.ds(pl.multiple_of(core * half + i * 16, 16), 16)
+        for start, size in runs(0, half):
+            r = pl.ds(start, size)
+            at = pl.ds(pl.multiple_of(core * half + start, 16), size)
             y = part_v[at, :].astype(F32) + got1[0, r, :].astype(F32) + far1[r, :].astype(F32)
             s = tok_v[at, :].astype(F32) + 0.5 * rms_value(y, gains[1:2, :])
             stream_v[r, :] = s
             mid_v[at, :] = rms_value(s, gains[2:3, :]).astype(BF16)
-            return carry
-
-        lax.fori_loop(0, half // 16, block, 0)
         sends.put(mid_v.at[mine, :], mid_v.at[mine, :], act_sem.at[2], partner)
 
     def into_pool(at):
@@ -749,55 +756,56 @@
             v = jnp.dot(rg_v[at, :], w, preferred_element_type=F32)
             partm_v[at, pl.ds(t * span, span)] = v.astype(BF16)
 
-    quarter = half // 2
+    units = half // 16
+    firsts = [-(-units * k // 3) * 16 for k in range(4)]
+    chunks = [(a, b - a) for a, b in zip(firsts[:-1], firsts[1:]) if b > a]
 
     def second_stream():
         arrived(gotm, act_sem.at[3])
-
-        def block(i, carry):
-            r = pl.ds(pl.multiple_of(i * 16, 16), 16)
-            at = pl.ds(pl.multiple_of(core * half + i * 16, 16), 16)
-            y = partm_v[at, :].astype(F32) + gotm[r, :].astype(F32)
-            s = stream_v[r, :] + rms_value(y, gains[3:4, :])
-            stream_v[r, :] = s
-            own_v[at, :] = rms_value(s, gains[4:5, :]).astype(BF16)
-            return carry
-
-        for k in range(2):
-            lax.fori_loop(k * quarter // 16, (k + 1) * quarter // 16, block, 0)
-            src = own_v.at[pl.ds(mo(core * half + k * quarter, 16), quarter), :]
-            sends.put(src, far_at(k, core), act_sem.at[4 + k], buddy)
+        for k, (first, count) in enumerate(chunks):
+            for start, size in runs(first, count):
+                r = pl.ds(start, size)
+                at = pl.ds(pl.multiple_of(core * half + start, 16), size)
+                y = partm_v[at, :].astype(F32) + gotm[r, :].astype(F32)
+                s = stream_v[r, :] + rms_value(y, gains[3:4, :])
+                stream_v[r, :] = s
+                own_v[at, :] = rms_value(s, gains[4:5, :]).astype(BF16)
+            src = own_v.at[pl.ds(mo(core * half + first, 16), count), :]
+            sends.put(src, far_at(k, core), act_sem.at[32 + k], buddy)
         sends.put(own_v.at[mine, :], own_v.at[mine, :], act_sem.at[6], partner)
 
+    def far_rows(k, c):
+        first, count = chunks[k]
+        return mo(2 * first + c * count, 16), count
+
     def far_at(k, c):
-        return far_v.at[pl.ds(mo((2 * k + c) * quarter, 16), quarter), :]
+        return far_v.at[pl.ds(*far_rows(k, c)), :]
 
     def far_on(k):
-        arrived(far_at(k, core), act_sem.at[4 + k])
-        sends.put(far_at(k, core), far_at(k, core), act_sem.at[20 + k], partner)
-
-    def down2(dst, base, count):
+        arrived(far_at(k, core), act_sem.at[32 + k])
+        sends.put(far_at(k, core), far_at(k, core), act_sem.at[36 + k], partner)
+
+    def down2(base, count, low, high):
         at = pl.ds(base, count)
 
         def body(t, carry):
             part2_v[at, pl.ds(pl.multiple_of(t * span, 128), span)] = down_block(t, at)
             return carry
 
-        lax.fori_loop(0, nz, body, 0)
+        lax.fori_loop(low, high, body, 0)
 
     def far_part(k, c):
-        return pl.ds(mo(rows + (2 * k + c) * quarter, 16), quarter)
+        first, count = far_rows(k, c)
+        return pl.ds(mo(rows + first, 16), count)
 
     last = len(steps)
     stage1(0)
-    for n in (1, 2, 3):
+    for n in range(2, 6):
         stage0(n)
+    stage1(1)
     mix_own()
     tokens_out()
-    stage0(5)
-    stage1(1)
     stage2(0)
-    mix_turn()
     all_mine = pl.ds(0, rows)
     all_far = pl.ds(rows, rows)
 
@@ -812,12 +820,16 @@
 
     for i in range(3 * nz):
         advance(i)
+        if i == 0:
+            mix_turn()
         if i == 2:
             tokens_on()
+            mix_up()
         if i == 4:
             first_norm()
-        if i == nz + 1:
-            mix_up()
+        for p in range(1, nz):
+            if i == 3 + 2 * p:
+                mix_on(p)
         if i == 2 * nz - 1:
             gate_up(norm_v, all_mine, all_mine)
         if i == 2 * nz:
@@ -825,15 +837,11 @@
         if i == 2 * nz + 1:
             down1(0)
             down1(1)
-            mix_on(1)
         if 2 * nz + 1 < i:
             down1(i - 2 * nz)
             if i == 2 * nz + 2:
                 reduce1(0)
-                mix_on(2)
             reduce1(i - 2 * nz - 1)
-    for p in range(3, nz):
-        mix_on(p)
     advance(3 * nz)
     reduce1(nz - 1)
     for i in range(3 * nz + 1, last - 1):
@@ -853,33 +861,31 @@
 
     arrived(own_v.at[theirs, :], act_sem.at[6])
     gate_up(own_v, all_mine, all_mine)
-    down2(own_v, 0, rows)
+    down2(0, rows, 0, nz // 2)
+    far_on(0)
+    down2(0, rows, nz // 2, nz)
     sends.put(part2_v.at[theirs, :], got2o, act_sem.at[7], partner)
-    for k in range(2):
-        far_on(k)
-        arrived(far_at(k, 1 - core), act_sem.at[20 + k])
-        base = 2 * k * quarter
-        gate_up(far_v, pl.ds(base, 2 * quarter), pl.ds(rows + base, 2 * quarter))
-        down2(far_v, rows + base, 2 * quarter)
-        sends.put(part2_v.at[far_part(k, 1 - core), :], got2f.at[k], act_sem.at[22 + k], partner)
-        arrived(got2f.at[k], act_sem.at[22 + k])
-        total = part2_v[far_part(k, core), :].astype(F32) + got2f[k].astype(F32)
-        sum2[k] = total.astype(BF16)
-        there = far2.at[pl.ds(k * quarter, quarter), :]
-        sends.put(sum2.at[k], there, act_sem.at[24 + k], buddy)
+    for k, (first, count) in enumerate(chunks):
+        arrived(far_at(k, 1 - core), act_sem.at[36 + k])
+        here = pl.ds(first, count)
+        gate_up(far_v, pl.ds(2 * first, 2 * count), pl.ds(rows + 2 * first, 2 * count))
+        if k + 1 < len(chunks):
+            far_on(k + 1)
+        down2(rows + 2 * first, 2 * count, 0, nz)
+        sends.put(part2_v.at[far_part(k, 1 - core), :], got2f.at[here, :], act_sem.at[40 + k], partner)
+        arrived(got2f.at[here, :], act_sem.at[40 + k])
+        total = part2_v[far_part(k, core), :].astype(F32) + got2f[here, :].astype(F32)
+        sum2[here, :] = total.astype(BF16)
+        sends.put(sum2.at[here, :], far2.at[here, :], act_sem.at[44 + k], buddy)
     arrived(got2o, act_sem.at[7])
-
-    def last_block(i, carry):
-        r = pl.ds(pl.multiple_of(i * 16, 16), 16)
-        at = pl.ds(pl.multiple_of(core * half + i * 16, 16), 16)
-        y = part2_v[at, :].astype(F32) + got2o[r, :].astype(F32) + far2[r, :].astype(F32)
-        s = stream_v[r, :] + 0.5 * rms_value(y, gains[5:6, :])
-        out_v[r, :] = s.astype(BF16)
-        return carry
-
-    for k in range(2):
-        arrived(far2.at[pl.ds(k * quarter, quarter), :], act_sem.at[24 + k])
-        lax.fori_loop(k * quarter // 16, (k + 1) * quarter // 16, last_block, 0)
+    for k, (first, count) in enumerate(chunks):
+        arrived(far2.at[pl.ds(first, count), :], act_sem.at[44 + k])
+        for start, size in runs(first, count):
+            r = pl.ds(start, size)
+            at = pl.ds(pl.multiple_of(core * half + start, 16), size)
+            y = part2_v[at, :].astype(F32) + got2o[r, :].astype(F32) + far2[r, :].astype(F32)
+            s = stream_v[r, :] + 0.5 * rms_value(y, gains[5:6, :])
+            out_v[r, :] = s.astype(BF16)
     final = pltpu.make_async_copy(out_v, out, local_sem.at[2])
     final.start()
     sends.drain()
@@ -918,10 +924,10 @@
         buf(rows, feat),
         buf(2, half, feat),
         buf(half, feat),
-        buf(2, half // 2, feat),
         buf(half, feat),
         buf(half, feat),
-        buf(2, half // 2, feat),
+        buf(half, feat),
+        buf(half, feat),
         buf(half, feat),
         buf(half, feat),
         buf(half, feat, dtype=F32),
@@ -932,7 +938,7 @@
         pltpu.SemaphoreType.DMA((SENDS,)),
         pltpu.SemaphoreType.DMA((4, count, 2)),
         pltpu.SemaphoreType.DMA((count,)),
-        pltpu.SemaphoreType.DMA((32,)),
+        pltpu.SemaphoreType.DMA((48,)),
         pltpu.SemaphoreType.DMA((4,)),
         pltpu.SemaphoreType.DMA((4, 2)),
     ]

time: 239 us -> 217 us (0.908)
  the two profiles are of different devices: /device:TPU:19 before, /device:TPU:0 now
where the time goes in v2:
time: 217 us; the launch traced here: 216 us
  Pallas kernels  213 us (98%)
    pallas_call x1, Pallas kernels, whole_layer(): pl.pallas_call(functools.partial(layer_kernel, dims), out_shape=jax.Shape...  213 us

profile of v2, /device:TPU:0, one launch (start us, length us, event | category | flops | bytes accessed | tf_op | source)
XLA Modules:
  0.0 216.5 jit_solution(7360175626622652159)
XLA Ops:
  0.0 1.3 reshape.7
  1.3 213.2 %whole_layer.1 = bf16[160,2048]{1,0:T(8,128)(2,1)} custom-call(bf16[320,2048]{1,0:T(8,128)(2,1)} %refs_0_.1, bf16[128,2816]{1,0:T(8,128)(2,1)} %refs_1_.1, bf16[128,2816]{1,0:T(8,128)(2,1)} %refs_2_.1, bf16[2816,128]{1,0:T(8,128)(2,1)} %refs_3_.1, bf16[128,512]{1,0:T(8,128)(2,1)} %refs_4_.1, bf16[512,128]{1,0:T(8,128)(2,1)} %refs_5_.1, ...), custom_call_target="tpu_custom_call" | custom-call | tf_op jit(solution)/shard_map/whole_layer/pallas_call | solution.py:947
  214.5 2.0 copy.11

commit v3 on v2

--- a/solution.py
+++ b/solution.py
@@ -460,28 +460,34 @@
 
 class Sends:
     def __init__(self, sem):
-        self.sem, self.count, self.pending = sem, 0, []
+        self.sem, self.count, self.pending = sem, 0, {}
 
     def put(self, src, dst, recv, to, ok=None):
+        slot = self.count % SENDS
+        self.count += 1
+        self.settle(slot)
         copy = pltpu.make_async_remote_copy(
             src_ref=src,
             dst_ref=dst,
-            send_sem=self.sem.at[self.count],
+            send_sem=self.sem.at[slot],
             recv_sem=recv,
             device_id=to,
             device_id_type=MESH,
         )
-        self.count += 1
         when(ok, copy.start)
-        self.pending.append((ok, copy))
+        self.pending[slot] = (ok, copy)
+
+    def settle(self, slot):
+        if slot in self.pending:
+            ok, copy = self.pending.pop(slot)
+            when(ok, copy.wait_send)
 
     def drain(self):
-        for ok, copy in self.pending:
-            when(ok, copy.wait_send)
-        self.pending = []
-
-
-SENDS = 192
+        for slot in list(self.pending):
+            self.settle(slot)
+
+
+SENDS = 96
 F32, BF16 = jnp.float32, jnp.bfloat16
 
 
@@ -555,14 +561,19 @@
     def pieces(m):
         return range(2) if m < 3 else range(1)
 
+    tall = mix_out.shape[0]
+    early = tall // 4
+    late_rows = pl.ds(0, tall - early)
+    early_rows = pl.ds(tall - early, early)
+
     def spot(m, src, u):
-        return place(m, src, u) if m < 3 else mout_v.at[src]
+        return place(m, src, u) if m < 3 else mout_v.at[src, late_rows, :]
 
     def sem_of(m, src, u):
-        return ff_sem.at[m, src, u]
+        return ff_sem.at[m, src]
 
     def origin(m, h, u):
-        return own_piece(m, h, u) if m < 3 else mix_out
+        return own_piece(m, h, u) if m < 3 else mix_out.at[late_rows, :]
 
     def stage0(n):
         m, p = steps[n]
@@ -575,14 +586,23 @@
     def stage1(n):
         m, p = steps[n]
         src = plane(p) * sz + col
+        if p:
+            came(m, src)
         for u in pieces(m):
-            if p:
-                arrived(spot(m, src, u), sem_of(m, src, u))
             for nb in (xn, yn):
                 first = spot(m, src, u) if p else origin(m, z % 2, u)
                 sends.put(first, spot(m, src, u), sem_of(m, src, u), {"fs": nb})
             if not p:
-                local((m, u), origin(m, z % 2, u), spot(m, me, u), loc_ff.at[m, u])
+                key = local_sem.at[0] if m == 3 else loc_ff.at[m, u]
+                local((m, u), origin(m, z % 2, u), spot(m, me, u), key)
+
+    def shard(m, src):
+        if m < 2:
+            return weights[m][1].at[pl.ds(mo(src * depth, 16), depth), :]
+        return down_v.at[src] if m < 3 else spot(m, src, 0)
+
+    def came(m, src):
+        arrived(shard(m, src), ff_sem.at[m, src])
 
     def three(p):
         shift = plane(p) * sz - z * sz
@@ -591,7 +611,7 @@
     def relay(m, p, u, across):
         a, b, _ = three(p)
         src, to = (a, yn) if across else (b, xn)
-        arrived(spot(m, src, u), sem_of(m, src, u))
+        came(m, src)
         sends.put(spot(m, src, u), spot(m, src, u), sem_of(m, src, u), {"fs": to})
 
     def stage2(n):
@@ -605,48 +625,55 @@
     def stage3(n):
         m, p = steps[n]
         a, b, d = three(p)
-        if m < 3:
-            todo = [(a, 1), (b, 0), (d, 0), (d, 1)]
-        else:
-            todo = [(b if p % 2 == 0 else a, 0), (d, 0)]
-        for src, u in todo:
-            arrived(spot(m, src, u), sem_of(m, src, u))
+        if m == 3:
+            came(m, b if p % 2 == 0 else a)
+        came(m, d)
         if p == 0:
             for u in pieces(m):
                 locals_[(m, u)].wait()
 
-    def min_at(src):
-        return min_v.at[pl.ds(mo(src * depth, 16), depth), :]
+    def mix_at(k, src):
+        if k == 0:
+            return min_v.at[pl.ds(mo(src * depth, 16), depth), :]
+        return mout_v.at[src, early_rows, :]
+
+    mixes = (mix_in, mix_out.at[early_rows, :])
 
     def mix_own():
-        for nb in (xn, yn):
-            sends.put(mix_in, min_at(me), mix_sem.at[me], {"fs": nb})
-        local("mix", mix_in, min_at(me), local_sem.at[0])
+        for k, ref in enumerate(mixes):
+            for nb in (xn, yn):
+                sends.put(ref, mix_at(k, me), mix_sem.at[k, me], {"fs": nb})
+            local(("mix", k), ref, mix_at(k, me), loc_ff.at[3, k])
 
     def mix_turn():
-        arrived(min_at(xn), mix_sem.at[xn])
-        sends.put(min_at(xn), min_at(xn), mix_sem.at[xn], {"fs": yn})
+        for k, (src, to) in enumerate(((xn, yn), (yn, xn))):
+            arrived(mix_at(k, src), mix_sem.at[k, src])
+            sends.put(mix_at(k, src), mix_at(k, src), mix_sem.at[k, src], {"fs": to})
 
     def mix_up():
-        arrived(min_at(yn), mix_sem.at[yn])
-        arrived(min_at(dg), mix_sem.at[dg])
-        locals_["mix"].wait()
-        for src in (me, xn, yn, dg):
-            for step in (1, -1):
-                ok = jnp.logical_and(z + step >= 0, z + step < nz)
-                sends.put(min_at(src), min_at(src), mix_sem.at[src], {"fs": me + step * sz}, ok)
+        for k, src in enumerate((yn, xn)):
+            arrived(mix_at(k, src), mix_sem.at[k, src])
+        for k in range(2):
+            arrived(mix_at(k, dg), mix_sem.at[k, dg])
+            locals_[("mix", k)].wait()
+            for src in (me, xn, yn, dg):
+                here = mix_at(k, src)
+                for step in (1, -1):
+                    ok = jnp.logical_and(z + step >= 0, z + step < nz)
+                    sends.put(here, here, mix_sem.at[k, src], {"fs": me + step * sz}, ok)
 
     def mix_on(p, forward=True):
         found, away = near(z, nz, p)
         shift = (found - z) * sz
         inside = jnp.logical_and(z + away >= 0, z + away < nz)
-        for src in (me + shift, xn + shift, yn + shift, dg + shift):
-            here, sem = min_at(src), mix_sem.at[src]
-            if forward:
-                when(inside, functools.partial(arrived, here, sem))
-                sends.put(here, here, sem, {"fs": me + away * sz}, inside)
-            else:
-                when(jnp.logical_not(inside), functools.partial(arrived, here, sem))
+        for k in range(2):
+            for src in (me + shift, xn + shift, yn + shift, dg + shift):
+                here, sem = mix_at(k, src), mix_sem.at[k, src]
+                if forward:
+                    when(inside, functools.partial(arrived, here, sem))
+                    sends.put(here, here, sem, {"fs": me + away * sz}, inside)
+                else:
+                    when(jnp.logical_not(inside), functools.partial(arrived, here, sem))
 
     mine = pl.ds(mo(core * half, 16), half)
     theirs = pl.ds(mo((1 - core) * half, 16), half)
@@ -692,34 +719,51 @@
         if hid % 256:
             tile(pl.ds(whole * 256, hid % 256), hid % 256)
 
-    def down_block(t, at):
-        w = jnp.concatenate([down_v[t * sz + i] for i in range(sz)], axis=1)
+    def down_block(first, many, at):
+        w = jnp.concatenate([down_v[first + i] for i in range(many)], axis=1)
         return jnp.dot(hid_v[at, :], w, preferred_element_type=F32).astype(BF16)
 
-    def cols_of(t):
-        return pl.ds(mo(t * span, 128), span)
-
-    def down1(p):
-        t = plane(p)
-        cols = cols_of(t)
+    def cols_of(first, many):
+        return pl.ds(mo(first * wide, 128), many * wide)
+
+    def down1(first, many, sem):
+        cols = cols_of(first, many)
         for i, (base, other) in enumerate(((rows, theirs_far), (0, theirs))):
             at = pl.ds(base, rows)
-            part_v[at, cols] = down_block(t, at)
-            sends.put(part_v.at[other, cols], got1.at[1 - i, :, cols], act_sem.at[8 + 2 * p + i], partner)
-
-    def reduce1(p):
-        cols = cols_of(plane(p))
+            part_v[at, cols] = down_block(first, many, at)
+            sends.put(part_v.at[other, cols], got1.at[1 - i, :, cols], act_sem.at[sem + i], partner)
+
+    def reduce1(first, many, sem):
+        cols = cols_of(first, many)
         for i in range(2):
-            arrived(got1.at[1 - i, :, cols], act_sem.at[8 + 2 * p + i])
+            arrived(got1.at[1 - i, :, cols], act_sem.at[sem + i])
         total = part_v[mine_far, cols].astype(F32) + got1[1, :, cols].astype(F32)
         sum1[:, cols] = total.astype(BF16)
-        sends.put(sum1.at[:, cols], far1.at[:, cols], act_sem.at[16 + plane(p)], buddy)
+        sends.put(sum1.at[:, cols], far1.at[:, cols], sum_sem(first, many), buddy)
+
+    row_y = (me // sy) % 2
+
+    def near_pair(p):
+        return plane(p) * sz + row_y * sy
+
+    def far_pair(p):
+        return plane(p) * sz + (1 - row_y) * sy
+
+    def sum_sem(first, many):
+        t = first // sz
+        return act_sem.at[29 + 2 * t + ((first // sy) % 2 if many < sz else 0)]
 
     def first_stream():
-        for t in range(nz):
-            cols = cols_of(t)
-            arrived(far1.at[:, cols], act_sem.at[16 + t])
-
+        buddy_z = z + sign
+        for p in range(nz):
+            t = near(buddy_z, nz, p)[0] if p else buddy_z
+            if p < nz - 1:
+                cols = cols_of(t * sz, sz)
+                arrived(far1.at[:, cols], sum_sem(t * sz, sz))
+            else:
+                for k in range(2):
+                    cols = cols_of(t * sz + k * sy, sy)
+                    arrived(far1.at[:, cols], sum_sem(t * sz + k * sy, sy))
         for start, size in runs(0, half):
             r = pl.ds(start, size)
             at = pl.ds(pl.multiple_of(core * half + start, 16), size)
@@ -747,7 +791,8 @@
                 k *= 2
             count = jnp.minimum(t + 1, window).astype(F32)
             dev = (total / count - v).astype(BF16)
-            o = jnp.dot(dev, pool_w[g], preferred_element_type=F32) * pool_scale[:, cols]
+            o = jnp.dot(dev, pool_w[g], preferred_element_type=F32)
+            o = o * pool_scale[cols].astype(F32).reshape(1, dim)
             rg_v[:, cols] = o.astype(BF16)
 
     def out_pool(at):
@@ -757,12 +802,13 @@
             partm_v[at, pl.ds(t * span, span)] = v.astype(BF16)
 
     units = half // 16
-    firsts = [-(-units * k // 3) * 16 for k in range(4)]
+    most = -(-units * 2 // 5)
+    firsts = [min(most * k, units) * 16 for k in range(4)]
     chunks = [(a, b - a) for a, b in zip(firsts[:-1], firsts[1:]) if b > a]
 
     def second_stream():
-        arrived(gotm, act_sem.at[3])
         for k, (first, count) in enumerate(chunks):
+            arrived(gotm.at[pl.ds(first, count), :], act_sem.at[14 + k])
             for start, size in runs(first, count):
                 r = pl.ds(start, size)
                 at = pl.ds(pl.multiple_of(core * half + start, 16), size)
@@ -771,8 +817,8 @@
                 stream_v[r, :] = s
                 own_v[at, :] = rms_value(s, gains[4:5, :]).astype(BF16)
             src = own_v.at[pl.ds(mo(core * half + first, 16), count), :]
-            sends.put(src, far_at(k, core), act_sem.at[32 + k], buddy)
-        sends.put(own_v.at[mine, :], own_v.at[mine, :], act_sem.at[6], partner)
+            sends.put(src, far_at(k, core), act_sem.at[17 + k], buddy)
+            sends.put(src, src, act_sem.at[29 + 2 * nz + k], partner)
 
     def far_rows(k, c):
         first, count = chunks[k]
@@ -782,14 +828,14 @@
         return far_v.at[pl.ds(*far_rows(k, c)), :]
 
     def far_on(k):
-        arrived(far_at(k, core), act_sem.at[32 + k])
-        sends.put(far_at(k, core), far_at(k, core), act_sem.at[36 + k], partner)
+        arrived(far_at(k, core), act_sem.at[17 + k])
+        sends.put(far_at(k, core), far_at(k, core), act_sem.at[20 + k], partner)
 
     def down2(base, count, low, high):
         at = pl.ds(base, count)
 
         def body(t, carry):
-            part2_v[at, pl.ds(pl.multiple_of(t * span, 128), span)] = down_block(t, at)
+            part2_v[at, pl.ds(pl.multiple_of(t * span, 128), span)] = down_block(t * sz, sz, at)
             return carry
 
         lax.fori_loop(low, high, body, 0)
@@ -806,90 +852,124 @@
     mix_own()
     tokens_out()
     stage2(0)
+    stage2(1)
     all_mine = pl.ds(0, rows)
     all_far = pl.ds(rows, rows)
 
+    z_order = {0: (6, 7), 2: (9,), 3: (10, 11)}
+    z_order.update({2 * nz - 1 + k: (3 * nz + 1 + k,) for k in range(nz - 1)})
+
     def advance(i):
-        if i + 6 < last:
-            stage0(i + 6)
+        for n in z_order.get(i, ()):
+            stage0(n)
         if i + 2 < last:
             stage1(i + 2)
-        if i + 1 < last:
+        if 0 < i < last - 1:
             stage2(i + 1)
         stage3(i)
 
-    for i in range(3 * nz):
+    final = 3 * nz - 1
+    for i in range(final):
         advance(i)
         if i == 0:
             mix_turn()
+        if i == 1:
+            mix_up()
         if i == 2:
             tokens_on()
-            mix_up()
         if i == 4:
             first_norm()
-        for p in range(1, nz):
-            if i == 3 + 2 * p:
-                mix_on(p)
+        for p, when_on in enumerate((5, 6)):
+            if i == when_on:
+                mix_on(p + 1)
         if i == 2 * nz - 1:
             gate_up(norm_v, all_mine, all_mine)
         if i == 2 * nz:
             gate_up(norm_v, all_far, all_far)
+            for p in range(3, nz):
+                mix_on(p)
+            down1(plane(0) * sz, sz, 4)
         if i == 2 * nz + 1:
-            down1(0)
-            down1(1)
-        if 2 * nz + 1 < i:
-            down1(i - 2 * nz)
-            if i == 2 * nz + 2:
-                reduce1(0)
-            reduce1(i - 2 * nz - 1)
-    advance(3 * nz)
-    reduce1(nz - 1)
-    for i in range(3 * nz + 1, last - 1):
-        advance(i)
-    first_stream()
+            down1(plane(1) * sz, sz, 6)
+            reduce1(plane(0) * sz, sz, 4)
+        if i == 2 * nz + 2:
+            down1(plane(2) * sz, sz, 8)
+            reduce1(plane(1) * sz, sz, 6)
+    late = range(3 * nz, last)
+    for n in late[2:]:
+        stage1(n - 1)
+    stage1(last - 1)
+    stage2(late[0])
+    d = three(nz - 1)[2]
+    down1(near_pair(nz - 1), sy, 10)
+    reduce1(plane(2) * sz, sz, 8)
+    came(2, d)
+    down1(far_pair(nz - 1), sy, 12)
+    reduce1(near_pair(nz - 1), sy, 10)
+    stage2(late[1])
+    reduce1(far_pair(nz - 1), sy, 12)
+    for n in late[2:]:
+        stage2(n)
     for p in range(1, nz):
         mix_on(p, forward=False)
+    first_stream()
     into_pool(mine)
     arrived(mid_v.at[theirs, :], act_sem.at[2])
     into_pool(theirs)
     pool()
-    advance(last - 1)
+    for n in late:
+        stage3(n)
     out_pool(theirs)
-    sends.put(partm_v.at[theirs, :], gotm, act_sem.at[3], partner)
+    for k, (first, count) in enumerate(chunks):
+        src = partm_v.at[pl.ds(mo((1 - core) * half + first, 16), count), :]
+        sends.put(src, gotm.at[pl.ds(first, count), :], act_sem.at[14 + k], partner)
     out_pool(mine)
     second_stream()
 
-    arrived(own_v.at[theirs, :], act_sem.at[6])
-    gate_up(own_v, all_mine, all_mine)
-    down2(0, rows, 0, nz // 2)
-    far_on(0)
-    down2(0, rows, nz // 2, nz)
-    sends.put(part2_v.at[theirs, :], got2o, act_sem.at[7], partner)
-    for k, (first, count) in enumerate(chunks):
-        arrived(far_at(k, 1 - core), act_sem.at[36 + k])
-        here = pl.ds(first, count)
+    def far_product(k):
+        first, count = chunks[k]
+        arrived(far_at(k, 1 - core), act_sem.at[20 + k])
         gate_up(far_v, pl.ds(2 * first, 2 * count), pl.ds(rows + 2 * first, 2 * count))
-        if k + 1 < len(chunks):
+        if 0 < k < len(chunks) - 1:
             far_on(k + 1)
         down2(rows + 2 * first, 2 * count, 0, nz)
-        sends.put(part2_v.at[far_part(k, 1 - core), :], got2f.at[here, :], act_sem.at[40 + k], partner)
-        arrived(got2f.at[here, :], act_sem.at[40 + k])
+        here = got2f.at[pl.ds(first, count), :]
+        sends.put(part2_v.at[far_part(k, 1 - core), :], here, act_sem.at[23 + k], partner)
+
+    def far_sum(k):
+        here = pl.ds(*chunks[k])
+        arrived(got2f.at[here, :], act_sem.at[23 + k])
         total = part2_v[far_part(k, core), :].astype(F32) + got2f[here, :].astype(F32)
         sum2[here, :] = total.astype(BF16)
-        sends.put(sum2.at[here, :], far2.at[here, :], act_sem.at[44 + k], buddy)
-    arrived(got2o, act_sem.at[7])
+        sends.put(sum2.at[here, :], far2.at[here, :], act_sem.at[26 + k], buddy)
+
     for k, (first, count) in enumerate(chunks):
-        arrived(far2.at[pl.ds(first, count), :], act_sem.at[44 + k])
+        here = pl.ds(mo((1 - core) * half + first, 16), count)
+        arrived(own_v.at[here, :], act_sem.at[29 + 2 * nz + k])
+    gate_up(own_v, all_mine, all_mine)
+    far_on(0)
+    down2(0, rows, 0, nz // 2)
+    far_product(0)
+    far_on(1)
+    down2(0, rows, nz // 2, nz)
+    sends.put(part2_v.at[theirs, :], got2o, act_sem.at[3], partner)
+    far_sum(0)
+    for k in range(1, len(chunks)):
+        far_product(k)
+        far_sum(k)
+    arrived(got2o, act_sem.at[3])
+    for k, (first, count) in enumerate(chunks):
+        arrived(far2.at[pl.ds(first, count), :], act_sem.at[26 + k])
         for start, size in runs(first, count):
             r = pl.ds(start, size)
             at = pl.ds(pl.multiple_of(core * half + start, 16), size)
             y = part2_v[at, :].astype(F32) + got2o[r, :].astype(F32) + far2[r, :].astype(F32)
             s = stream_v[r, :] + 0.5 * rms_value(y, gains[5:6, :])
             out_v[r, :] = s.astype(BF16)
-    final = pltpu.make_async_copy(out_v, out, local_sem.at[2])
-    final.start()
+    leave = pltpu.make_async_copy(out_v, out, local_sem.at[2])
+    leave.start()
     sends.drain()
-    final.wait()
+    leave.wait()
 
 
 def whole_layer(dims, tokens, w_gate, w_up, w_down, w_mix_in, w_mix_out, pool_w, pool_scale, gains):
@@ -903,7 +983,6 @@
     half = rows // 2
     wide = w_down.shape[1]
     pooled = w_mix_in.shape[1]
-    scale = pool_scale.astype(F32).reshape(1, -1)
 
     def buf(*shape, dtype=BF16):
         return pltpu.VMEM(shape, dtype)
@@ -936,9 +1015,9 @@
         buf(rows, pooled),
         buf(half, feat),
         pltpu.SemaphoreType.DMA((SENDS,)),
-        pltpu.SemaphoreType.DMA((4, count, 2)),
-        pltpu.SemaphoreType.DMA((count,)),
-        pltpu.SemaphoreType.DMA((48,)),
+        pltpu.SemaphoreType.DMA((4, count)),
+        pltpu.SemaphoreType.DMA((2, count)),
+        pltpu.SemaphoreType.DMA((32 + 2 * nz,)),
         pltpu.SemaphoreType.DMA((4,)),
         pltpu.SemaphoreType.DMA((4, 2)),
     ]
@@ -954,7 +1033,7 @@
             collective_id=1, has_side_effects=True, vmem_limit_bytes=67043328
         ),
         name="whole_layer",
-    )(tokens, w_gate, w_up, w_down, w_mix_in, w_mix_out, pool_w, scale, gains)
+    )(tokens, w_gate, w_up, w_down, w_mix_in, w_mix_out, pool_w, pool_scale, gains)
 
 
 def paired(dims, mesh):

time: 217 us -> 207 us (0.954)
  Pallas kernels: 213 us -> 205 us
    pallas_call x1, Pallas kernels: 213 us -> 205 us  [whole_layer(): pl.pallas_call(functools.partial(layer_kernel, dims), out_shape=jax.Shape...]
where the time goes in v3:
time: 207 us
  Pallas kernels  205 us (99%)
    pallas_call x1, Pallas kernels, whole_layer(): pl.pallas_call(functools.partial(layer_kernel, dims), out_shape=jax.Shape...  205 us

profile of v3, /device:TPU:0, one launch (start us, length us, event | category | flops | bytes accessed | tf_op | source)
XLA Modules:
  0.0 206.9 jit_solution(4421156409488056685)
XLA Ops:
  0.0 204.9 %whole_layer.1 = bf16[160,2048]{1,0:T(8,128)(2,1)} custom-call(bf16[320,2048]{1,0:T(8,128)(2,1)} %refs_0_.1, bf16[128,2816]{1,0:T(8,128)(2,1)} %refs_1_.1, bf16[128,2816]{1,0:T(8,128)(2,1)} %refs_2_.1, bf16[2816,128]{1,0:T(8,128)(2,1)} %refs_3_.1, bf16[128,512]{1,0:T(8,128)(2,1)} %refs_4_.1, bf16[512,128]{1,0:T(8,128)(2,1)} %refs_5_.1, ...), custom_call_target="tpu_custom_call" | custom-call | tf_op jit(solution)/shard_map/whole_layer/pallas_call | solution.py:1026
  204.9 2.0 copy.11

commit v4 on v3

--- a/solution.py
+++ b/solution.py
@@ -487,17 +487,18 @@
             self.settle(slot)
 
 
-SENDS = 96
+SENDS = 48
 F32, BF16 = jnp.float32, jnp.bfloat16
 
 
 def layer_kernel(dims, *refs):
-    (tokens, gate, up, down, mix_in, mix_out, pool_w, pool_scale, gains, out) = refs[:10]
+    (tokens, gate, up, down, mix_in, mix_out, pool_far, scale_far, gains_far, out) = refs[:10]
     (gate_v, up_v, down_v, min_v, mout_v) = refs[10:15]
     (tok_v, norm_v, own_v, far_v, hid_v, part_v, part2_v, partm_v) = refs[15:23]
     (got1, got2o, got2f, gotm, sum1, sum2, far1, far2) = refs[23:31]
     (stream_v, mid_v, pin_v, rg_v, out_v) = refs[31:36]
-    (send_sem, ff_sem, mix_sem, act_sem, local_sem, loc_ff) = refs[36:]
+    (pool_w, pool_scale, gains) = refs[36:39]
+    (send_sem, ff_sem, mix_sem, act_sem, local_sem, loc_ff) = refs[39:]
     (nz, sz), (_, sy), (_, sx) = dims
     me, core = lax.axis_index("fs"), lax.axis_index("tp")
     z = me // sz
@@ -685,6 +686,9 @@
     def tokens_out():
         sends.put(tokens.at[mine, :], tok_v.at[mine_far, :], act_sem.at[0], buddy)
         local("tok", tokens, tok_v.at[pl.ds(0, rows), :], local_sem.at[1])
+        small = ((pool_far, pool_w), (scale_far, pool_scale), (gains_far, gains))
+        for k, (src, dst) in enumerate(small):
+            local(("small", k), src, dst, local_sem.at[5 + k])
 
     def tokens_on():
         here = tok_v.at[mine_far, :]
@@ -694,6 +698,8 @@
     def first_norm():
         arrived(tok_v.at[theirs_far, :], act_sem.at[1])
         locals_["tok"].wait()
+        for k in range(3):
+            locals_[("small", k)].wait()
 
         def block(i, carry):
             at = pl.ds(pl.multiple_of(i * 32, 32), 32)
@@ -703,21 +709,21 @@
 
         lax.fori_loop(0, 2 * rows // 32, block, 0)
 
-    def gate_up(src, at, dst):
+    tiles = hid // 256
+
+    def gate_up(src, at, dst, low=0, high=None):
         def tile(cols, n):
             w = jnp.concatenate([gate_v[:, cols], up_v[:, cols]], axis=1)
             both = jnp.dot(src[at, :], w, preferred_element_type=F32)
             hid_v[dst, cols] = (silu(both[:, :n]) * both[:, n:]).astype(BF16)
 
-        whole = hid // 256
-
         def body(j, carry):
             tile(pl.ds(pl.multiple_of(j * 256, 256), 256), 256)
             return carry
 
-        lax.fori_loop(0, whole, body, 0)
-        if hid % 256:
-            tile(pl.ds(whole * 256, hid % 256), hid % 256)
+        lax.fori_loop(low, tiles if high is None else high, body, 0)
+        if hid % 256 and high is None:
+            tile(pl.ds(tiles * 256, hid % 256), hid % 256)
 
     def down_block(first, many, at):
         w = jnp.concatenate([down_v[first + i] for i in range(many)], axis=1)
@@ -802,9 +808,15 @@
             partm_v[at, pl.ds(t * span, span)] = v.astype(BF16)
 
     units = half // 16
-    most = -(-units * 2 // 5)
-    firsts = [min(most * k, units) * 16 for k in range(4)]
+    firsts = [16 * k for k in (0, units * 3 // 10, units * 7 // 10, units)]
     chunks = [(a, b - a) for a, b in zip(firsts[:-1], firsts[1:]) if b > a]
+
+    def own_rows(k):
+        first, count = chunks[k]
+        return own_v.at[pl.ds(mo(core * half + first, 16), count), :]
+
+    def share(k):
+        sends.put(own_rows(k), far_at(k, core), act_sem.at[17 + k], buddy)
 
     def second_stream():
         for k, (first, count) in enumerate(chunks):
@@ -816,8 +828,9 @@
                 s = stream_v[r, :] + rms_value(y, gains[3:4, :])
                 stream_v[r, :] = s
                 own_v[at, :] = rms_value(s, gains[4:5, :]).astype(BF16)
-            src = own_v.at[pl.ds(mo(core * half + first, 16), count), :]
-            sends.put(src, far_at(k, core), act_sem.at[17 + k], buddy)
+            if k == 0:
+                share(0)
+            src = own_rows(k)
             sends.put(src, src, act_sem.at[29 + 2 * nz + k], partner)
 
     def far_rows(k, c):
@@ -929,8 +942,12 @@
     def far_product(k):
         first, count = chunks[k]
         arrived(far_at(k, 1 - core), act_sem.at[20 + k])
-        gate_up(far_v, pl.ds(2 * first, 2 * count), pl.ds(rows + 2 * first, 2 * count))
-        if 0 < k < len(chunks) - 1:
+        src, dst = pl.ds(2 * first, 2 * count), pl.ds(rows + 2 * first, 2 * count)
+        gate_up(far_v, src, dst, 0, tiles // 2)
+        if k:
+            far_sum(k - 1)
+        gate_up(far_v, src, dst, tiles // 2)
+        if k + 1 < len(chunks):
             far_on(k + 1)
         down2(rows + 2 * first, 2 * count, 0, nz)
         here = got2f.at[pl.ds(first, count), :]
@@ -946,17 +963,17 @@
     for k, (first, count) in enumerate(chunks):
         here = pl.ds(mo((1 - core) * half + first, 16), count)
         arrived(own_v.at[here, :], act_sem.at[29 + 2 * nz + k])
-    gate_up(own_v, all_mine, all_mine)
+    gate_up(own_v, all_mine, all_mine, 0, tiles // 2)
+    share(1)
+    gate_up(own_v, all_mine, all_mine, tiles // 2)
     far_on(0)
+    share(2)
     down2(0, rows, 0, nz // 2)
-    far_product(0)
-    far_on(1)
+    for k in range(len(chunks)):
+        far_product(k)
     down2(0, rows, nz // 2, nz)
     sends.put(part2_v.at[theirs, :], got2o, act_sem.at[3], partner)
-    far_sum(0)
-    for k in range(1, len(chunks)):
-        far_product(k)
-        far_sum(k)
+    far_sum(len(chunks) - 1)
     arrived(got2o, act_sem.at[3])
     for k, (first, count) in enumerate(chunks):
         arrived(far2.at[pl.ds(first, count), :], act_sem.at[26 + k])
@@ -966,10 +983,11 @@
             y = part2_v[at, :].astype(F32) + got2o[r, :].astype(F32) + far2[r, :].astype(F32)
             s = stream_v[r, :] + 0.5 * rms_value(y, gains[5:6, :])
             out_v[r, :] = s.astype(BF16)
-    leave = pltpu.make_async_copy(out_v, out, local_sem.at[2])
-    leave.start()
+        here = pl.ds(first, count)
+        local(("out", k), out_v.at[here, :], out.at[here, :], local_sem.at[2 + k])
     sends.drain()
-    leave.wait()
+    for k in range(len(chunks)):
+        locals_[("out", k)].wait()
 
 
 def whole_layer(dims, tokens, w_gate, w_up, w_down, w_mix_in, w_mix_out, pool_w, pool_scale, gains):
@@ -1014,19 +1032,21 @@
         buf(rows, pooled, dtype=F32),
         buf(rows, pooled),
         buf(half, feat),
+        buf(*pool_w.shape),
+        buf(*pool_scale.shape),
+        buf(*gains.shape, dtype=F32),
         pltpu.SemaphoreType.DMA((SENDS,)),
         pltpu.SemaphoreType.DMA((4, count)),
         pltpu.SemaphoreType.DMA((2, count)),
         pltpu.SemaphoreType.DMA((32 + 2 * nz,)),
-        pltpu.SemaphoreType.DMA((4,)),
+        pltpu.SemaphoreType.DMA((8,)),
         pltpu.SemaphoreType.DMA((4, 2)),
     ]
     hbm = pl.BlockSpec(memory_space=pltpu.HBM)
-    vmem = pl.BlockSpec(memory_space=pltpu.VMEM)
     return pl.pallas_call(
         functools.partial(layer_kernel, dims),
         out_shape=jax.ShapeDtypeStruct((half, feat), tokens.dtype),
-        in_specs=[hbm] * 6 + [vmem] * 3,
+        in_specs=[hbm] * 9,
         out_specs=hbm,
         scratch_shapes=scratch,
         compiler_params=pltpu.CompilerParams(

time: 207 us -> 204 us (0.986)
  Pallas kernels: 205 us -> 202 us
    pallas_call x1, Pallas kernels: 205 us -> 202 us  [whole_layer(): pl.pallas_call(functools.partial(layer_kernel, dims), out_shape=jax.Shape...]
where the time goes in v4:
time: 204 us
  Pallas kernels  202 us (99%)
    pallas_call x1, Pallas kernels, whole_layer(): pl.pallas_call(functools.partial(layer_kernel, dims), out_shape=jax.Shape...  202 us

profile of v4, /device:TPU:0, one launch (start us, length us, event | category | flops | bytes accessed | tf_op | source)
XLA Modules:
  0.0 204.3 jit_solution(14738284150937997170)
XLA Ops:
  0.0 202.3 %whole_layer.1 = bf16[160,2048]{1,0:T(8,128)(2,1)} custom-call(bf16[320,2048]{1,0:T(8,128)(2,1)} %refs_0_.1, bf16[128,2816]{1,0:T(8,128)(2,1)} %refs_1_.1, bf16[128,2816]{1,0:T(8,128)(2,1)} %refs_2_.1, bf16[2816,128]{1,0:T(8,128)(2,1)} %refs_3_.1, bf16[128,512]{1,0:T(8,128)(2,1)} %refs_4_.1, bf16[512,128]{1,0:T(8,128)(2,1)} %refs_5_.1, ...), custom_call_target="tpu_custom_call" | custom-call | tf_op jit(solution)/shard_map/whole_layer/pallas_call | solution.py:1046
  202.3 2.0 copy.11

commit v5 on v4

--- a/solution.py
+++ b/solution.py
@@ -869,8 +869,8 @@
     all_mine = pl.ds(0, rows)
     all_far = pl.ds(rows, rows)
 
-    z_order = {0: (6, 7), 2: (9,), 3: (10, 11)}
-    z_order.update({2 * nz - 1 + k: (3 * nz + 1 + k,) for k in range(nz - 1)})
+    z_order = {0: (6, 7), 2: (9,), 3: (10,), 4: (11,)}
+    z_order.update({nz + 1 + k: (3 * nz + 1 + k,) for k in range(nz - 1)})
 
     def advance(i):
         for n in z_order.get(i, ()):
@@ -919,8 +919,8 @@
     came(2, d)
     down1(far_pair(nz - 1), sy, 12)
     reduce1(near_pair(nz - 1), sy, 10)
+    reduce1(far_pair(nz - 1), sy, 12)
     stage2(late[1])
-    reduce1(far_pair(nz - 1), sy, 12)
     for n in late[2:]:
         stage2(n)
     for p in range(1, nz):

time: 204 us -> 204 us (level)
  no operation moved by 1% of the time
where the time goes in v5:
time: 204 us
  Pallas kernels  202 us (99%)
    pallas_call x1, Pallas kernels, whole_layer(): pl.pallas_call(functools.partial(layer_kernel, dims), out_shape=jax.Shape...  202 us

profile of v5, /device:TPU:0, one launch (start us, length us, event | category | flops | bytes accessed | tf_op | source)
XLA Modules:
  0.0 204.0 jit_solution(13882324436826009620)
XLA Ops:
  0.0 202.0 %whole_layer.1 = bf16[160,2048]{1,0:T(8,128)(2,1)} custom-call(bf16[320,2048]{1,0:T(8,128)(2,1)} %refs_0_.1, bf16[128,2816]{1,0:T(8,128)(2,1)} %refs_1_.1, bf16[128,2816]{1,0:T(8,128)(2,1)} %refs_2_.1, bf16[2816,128]{1,0:T(8,128)(2,1)} %refs_3_.1, bf16[128,512]{1,0:T(8,128)(2,1)} %refs_4_.1, bf16[512,128]{1,0:T(8,128)(2,1)} %refs_5_.1, ...), custom_call_target="tpu_custom_call" | custom-call | tf_op jit(solution)/shard_map/whole_layer/pallas_call | solution.py:1046
  202.1 2.0 copy.11
